TPU v7x, 256 devices: a 4x2x16 block of a 4x16x16 slice. The times are simulated.
256 devices in a mesh: grp: 2 (over y), tp: 16 (over z), dp: 8 (over x, core).
Axes of the slice: x: 4, y: 2, z: 16, core: 2. Of those that a mesh axis runs over, the one named last changes fastest.
The devices are a block of a 4x16x16 slice.
Arguments:
- tokens: bfloat16 [128, 8, 4096], P(('grp', 'tp'), None, 'dp'), parts along dimension 0, may hold values from -6 to 6
- lengths: int32 [128], P('grp'), parts along dimension 0, may hold values from 1 to 8, 224 in all
- norm_gain: float32 [2, 4096], P(None, 'dp'), may hold values from 0.1 to 1.9
- w_recept: bfloat16 [2, 4096, 2048], P(None, 'dp', 'tp'), may hold values from -0.09375 to 0.09375
- w_key: bfloat16 [2, 4096, 2048], P(None, 'dp', 'tp'), may hold values from -0.09375 to 0.09375
- w_value: bfloat16 [2, 4096, 2048], P(None, 'dp', 'tp'), may hold values from -0.09375 to 0.09375
- w_decay: bfloat16 [2, 4096, 2048], P(None, 'dp', 'tp'), may hold values from -0.375 to 0.375
- w_rate: bfloat16 [2, 4096, 2048], P(None, 'dp', 'tp'), may hold values from -0.09375 to 0.09375
- w_gate: bfloat16 [2, 4096, 2048], P(None, 'dp', 'tp'), may hold values from -0.09375 to 0.09375
- w_out: bfloat16 [2, 2048, 4096], P(None, 'tp', 'dp'), may hold values from -0.125 to 0.125
- decay_base: float32 [2, 2048], P(None, 'tp'), may hold values from -4 to 3
- out_gain: float32 [2, 2048], P(None, 'tp'), may hold values from 0.1 to 1.9
- states: float32 [2, 128, 64, 2048], P(None, ('grp', 'dp'), None, 'tp'), parts along dimension 1, may hold values from -6 to 6
Outputs:
- stream_out: float32 [128, 8, 4096], P(('grp', 'tp'), None, 'dp'), parts along dimension 0
- new_states: float32 [2, 128, 64, 2048], P(None, ('grp', 'dp'), None, 'tp'), parts along dimension 1
There are 2 independent parts, one for each index of `grp`. A program takes and returns all parts, laid end to end along the dimension named above; an argument that names none is the same for every part. Nothing has to cross between parts.
Inputs may be any that keep to these rules, and one draw needn't show every extreme that they name: lengths[b] first tokens of sequence b are live; together they count 7 * 32 and the largest is 8.
All inputs are finite; a program needn't handle non-finite values.
Results may differ from a plain program's by a relative error of at most 0.0061.
Values may be sent and summed in bfloat16 or wider, within the bound.
No kernel may reach another device: no remote copies, remote signals or barrier semaphores. Data moves between devices by JAX's collectives and lax.ppermute only.
A program may use at most 128 MiB of HBM per device.

v0:
```python
import jax
import jax.numpy as jnp
from jax import lax
from jax.sharding import Mesh
from jax.sharding import PartitionSpec as P

D = 4096
HEAD = 64
BLOCKS = 2
DP = ("dp_0", "dp_1")
GRP_DP = ("grp", "dp_0", "dp_1")


group_eps = 0.00064
norm_eps = 1e-06
key_eps = 1e-06
decay_scale = 0.606531
highest = lax.Precision.HIGHEST


def from_everyone(value, axis):
    size = lax.axis_size(axis)
    return lax.all_to_all(
        jnp.broadcast_to(value[None], (size, *value.shape)), axis, 0, 0, tiled=True
    )


def laid_out(blocks, dim):
    blocks = jnp.moveaxis(blocks, 0, dim)
    dims = blocks.shape
    return blocks.reshape(*dims[:dim], dims[dim] * dims[dim + 1], *dims[dim + 2 :])


def gather_directly(value, axis, dim):
    blocks = from_everyone(value, axis)
    return laid_out(blocks, dim)


def scatter_axes(value, axes, dim):
    for axis in axes:
        value = lax.psum_scatter(value, axis, scatter_dimension=dim, tiled=True)
    return value


def cut_along(value, dim, size):
    dims = value.shape
    blocks = value.reshape(*dims[:dim], size, dims[dim] // size, *dims[dim + 1 :])
    return jnp.moveaxis(blocks, dim, 0)


def sum_at_owner(value, axis, dim):
    size = lax.axis_size(axis)
    blocks = lax.all_to_all(cut_along(value, dim, size), axis, 0, 0, tiled=True)
    return jnp.sum(blocks, axis=0)


def mix_heads(
    state_in,
    recept,
    keys_in,
    values,
    decay_pre,
    rate_pre,
    gate_pre,
    base_shift,
    out_scale,
    live_mask,
    head_size,
):
    row_count, step_count, width_all = recept.shape
    head_count = width_all // head_size
    shape_heads = (row_count, step_count, head_count, head_size)
    decay_rate = jnp.exp(-decay_scale * jax.nn.sigmoid(decay_pre + base_shift)).reshape(shape_heads)
    learn_rate = jax.nn.sigmoid(rate_pre).reshape(shape_heads)
    key_heads = keys_in.reshape(shape_heads)
    unit_keys = key_heads * lax.rsqrt(
        jnp.sum(key_heads * key_heads, axis=3, keepdims=True) + key_eps
    )
    removal = unit_keys * learn_rate
    recept_heads = recept.reshape(shape_heads)
    value_heads = values.reshape(shape_heads)
    memory = state_in.reshape(row_count, head_size, head_count, head_size)
    outputs = []
    for position in range(step_count):
        seen_part = jnp.einsum("bihj,bhj->bhi", memory, unit_keys[:, position], precision=highest)
        updated = (
            memory * decay_rate[:, position][:, None, :, :]
            - jnp.swapaxes(seen_part, 1, 2)[:, :, :, None] * removal[:, position][:, None, :, :]
            + jnp.swapaxes(value_heads[:, position], 1, 2)[:, :, :, None]
            * key_heads[:, position][:, None, :, :]
        )
        memory = jnp.where(live_mask[:, position][:, None, None, None], updated, memory)
        outputs.append(
            jnp.einsum("bihj,bhj->bhi", memory, recept_heads[:, position], precision=highest)
        )
    readout = jnp.stack(outputs, axis=1)
    centered = readout - jnp.mean(readout, axis=3, keepdims=True)
    normed = centered * lax.rsqrt(jnp.mean(centered * centered, axis=3, keepdims=True) + group_eps)
    gated = normed.reshape(row_count, step_count, width_all) * out_scale * jax.nn.sigmoid(gate_pre)
    gated = jnp.where(live_mask[:, :, None], gated, 0.0)
    return (gated.astype(jnp.bfloat16), memory.reshape(row_count, head_size, width_all))


def body(
    tokens,
    lengths,
    norm_gain,
    w_recept,
    w_key,
    w_value,
    w_decay,
    w_rate,
    w_gate,
    w_out,
    decay_base,
    out_gain,
    states,
):
    horizon = tokens.shape[1]
    held_rows = states.shape[1]
    first_row = lax.axis_index(DP) * held_rows
    held_lengths = lax.dynamic_slice_in_dim(lengths, first_row, held_rows, 0)
    live_mask = jnp.arange(horizon, dtype=jnp.int32)[None, :] < held_lengths[:, None]
    current = tokens.astype(jnp.float32)
    finals = []
    for block_index in range(BLOCKS):
        gathered_in = gather_directly(current, "tp", 0)
        squares = jnp.sum(jnp.square(gathered_in), axis=2)
        total_squares = scatter_axes(squares, DP, 0)
        inv_rms = lax.rsqrt(total_squares / D + norm_eps)
        scaled = (gathered_in * norm_gain[block_index]).astype(jnp.bfloat16)
        partials = tuple(
            (
                jnp.einsum(
                    "bsd,dc->bsc", scaled, weight[block_index], preferred_element_type=jnp.float32
                )
                for weight in (w_recept, w_key, w_value, w_decay, w_rate, w_gate)
            )
        )
        summed = jax.tree.map(lambda part: sum_at_owner(part, DP, 0), partials)
        projected = [member * inv_rms[:, :, None] for member in summed]
        gated, final_state = mix_heads(
            states[block_index],
            projected[0],
            projected[1],
            projected[2],
            projected[3],
            projected[4],
            projected[5],
            decay_base[block_index],
            out_gain[block_index],
            live_mask,
            HEAD,
        )
        finals.append(final_state)
        all_rows = gather_directly(gated, DP, 0)
        regrouped = lax.all_to_all(all_rows, "tp", split_axis=0, concat_axis=2, tiled=True)
        output = jnp.einsum(
            "bsc,cd->bsd",
            regrouped,
            lax.all_gather(w_out[block_index], "tp", axis=0, tiled=True),
            preferred_element_type=jnp.float32,
        )
        current = current + output
    return (current, jnp.stack(finals, axis=0))


def solution(mesh):
    split = Mesh(
        mesh.devices.reshape(mesh.shape["grp"], mesh.shape["tp"], 4, 2),
        ("grp", "tp", "dp_0", "dp_1"),
    )
    return jax.shard_map(
        body,
        mesh=split,
        in_specs=(
            P(("grp", "tp"), None, DP),
            P("grp"),
            P(None, DP),
            P(None, DP, "tp"),
            P(None, DP, "tp"),
            P(None, DP, "tp"),
            P(None, DP, "tp"),
            P(None, DP, "tp"),
            P(None, DP, "tp"),
            P(None, "tp", DP),
            P(None, "tp"),
            P(None, "tp"),
            P(None, GRP_DP, None, "tp"),
        ),
        out_specs=(P(("grp", "tp"), None, DP), P(None, GRP_DP, None, "tp")),
        check_vma=False,
    )
```

profile of v0, /device:TPU:40, one launch (start us, length us, event | category | flops | bytes accessed | tf_op | source)
XLA Modules:
  0.0 620.5 jit_solution(10931402531203159044)
XLA Ops:
  9.9 24.1 %all-to-all-start = ((f32[16,4,8,512]{3,2,1,0:T(8,128)}), f32[16,4,8,512]{3,2,1,0:T(8,128)S(1)}, u32[]{:S(2)}, u32[]{:S(2)}) async-start(f32[16,4,8,512]{3,2,1,0:T(8,128)} %broadcast_in_dim.196), calls=%async_computation | async-start | bytes 2097152 | tf_op jit(solution)/shard_map/all_to_all | solution.py:23
  34.7 49.2 %all-to-all-done = f32[16,4,8,512]{3,2,1,0:T(8,128)S(1)} async-done(((f32[16,4,8,512]{3,2,1,0:T(8,128)}), f32[16,4,8,512]{3,2,1,0:T(8,128)S(1)}, u32[]{:S(2)}, u32[]{:S(2)}) %all-to-all-start) | async-done | bytes 1048608 | tf_op jit(solution)/shard_map/all_to_all | solution.py:23
  91.6 4.6 all-to-all-start.1
  97.2 6.5 %all-to-all-done.1 = f32[8,8,8,128]{3,2,1,0:T(8,128)S(1)} async-done(((f32[8,8,8,128]{3,2,1,0:T(8,128)}), f32[8,8,8,128]{3,2,1,0:T(8,128)S(1)}, u32[]{:S(2)}, u32[]{:S(2)}) %all-to-all-start.1) | async-done | bytes 262176 | tf_op jit(solution)/shard_map/all_to_all | solution.py:53
  103.8 3.6 all-to-all-start.5
  108.4 6.3 %all-to-all-done.5 = f32[8,8,8,128]{3,2,1,0:T(8,128)S(1)} async-done(((f32[8,8,8,128]{3,2,1,0:T(8,128)}), f32[8,8,8,128]{3,2,1,0:T(8,128)S(1)}, u32[]{:S(2)}, u32[]{:S(2)}) %all-to-all-start.5) | async-done | bytes 262176 | tf_op jit(solution)/shard_map/all_to_all | solution.py:53
  114.7 3.6 all-to-all-start.4
  119.3 6.3 %all-to-all-done.4 = f32[8,8,8,128]{3,2,1,0:T(8,128)S(1)} async-done(((f32[8,8,8,128]{3,2,1,0:T(8,128)}), f32[8,8,8,128]{3,2,1,0:T(8,128)S(1)}, u32[]{:S(2)}, u32[]{:S(2)}) %all-to-all-start.4) | async-done | bytes 262176 | tf_op jit(solution)/shard_map/all_to_all | solution.py:53
  125.6 3.6 all-to-all-start.3
  130.2 6.3 %all-to-all-done.3 = f32[8,8,8,128]{3,2,1,0:T(8,128)S(1)} async-done(((f32[8,8,8,128]{3,2,1,0:T(8,128)}), f32[8,8,8,128]{3,2,1,0:T(8,128)S(1)}, u32[]{:S(2)}, u32[]{:S(2)}) %all-to-all-start.3) | async-done | bytes 262176 | tf_op jit(solution)/shard_map/all_to_all | solution.py:53
  136.5 3.6 all-to-all-start.2
  141.2 2.6 all-reduce
  144.3 3.1 all-to-all-done.2
  147.4 4.4 all-to-all-start.6
  161.9 3.2 add_select_fusion.14
  170.4 4.7 add_select_fusion.13
  180.4 6.0 add_select_fusion.12
  191.0 7.2 %add_select_fusion.11 = f32[8,64,2,64]{3,2,1,0:T(2,128)S(1)} fusion(pred[8]{0:T(512)(128)(4,1)} %get-tuple-element.177, f32[8,2,64]{2,1,0:T(2,128)} %get-tuple-element.56, f32[8,64,2]{2,1,0:T(8,128)S(1)} %copy.60, f32[8,2,64]{2,1,0:T(2,128)} %get-tuple-element.41, f32[8,64,2]{2,1,0:T(8,128)S(1)} %bitcast.671, f32[8,2,64]{2,1,0:T(2,128)} %get-tuple-element.25, ...), kind=kLoop, calls=%fused_computation.52 | loop fusion | flops 1966080 | bytes 626728 | tf_op jit(solution)/shard_map/jit(_where)/select_n | solution.py:92
  202.9 8.8 %add_select_fusion.10 = f32[8,64,2,64]{3,2,1,0:T(2,128)S(1)} fusion(pred[8]{0:T(512)(128)(4,1)} %get-tuple-element.176, f32[8,2,64]{2,1,0:T(2,128)} %get-tuple-element.57, f32[8,64,2]{2,1,0:T(8,128)S(1)} %copy.61, f32[8,2,64]{2,1,0:T(2,128)} %get-tuple-element.42, f32[8,64,2]{2,1,0:T(8,128)} %bitcast.681, f32[8,2,64]{2,1,0:T(2,128)} %get-tuple-element.26, ...), kind=kLoop, calls=%fused_computation.51 | loop fusion | flops 2359296 | bytes 647216 | tf_op jit(solution)/shard_map/jit(_where)/select_n | solution.py:92
  216.3 9.7 %add_select_fusion.9 = f32[8,64,2,64]{3,2,1,0:T(2,128)S(1)} fusion(pred[8]{0:T(512)(128)(4,1)} %get-tuple-element.175, f32[8,2,64]{2,1,0:T(2,128)} %get-tuple-element.58, f32[8,64,2]{2,1,0:T(8,128)} %copy.62, f32[8,2,64]{2,1,0:T(2,128)} %get-tuple-element.43, f32[8,64,2]{2,1,0:T(8,128)} %bitcast.689, f32[8,2,64]{2,1,0:T(2,128)} %get-tuple-element.27, ...), kind=kLoop, calls=%fused_computation.50 | loop fusion | flops 2752512 | bytes 667704 | tf_op jit(solution)/shard_map/jit(_where)/select_n | solution.py:92
  236.1 11.1 %add_select_fusion.8 = f32[8,64,2,64]{3,2,1,0:T(2,128)S(1)} fusion(pred[8]{0:T(512)(128)(4,1)} %get-tuple-element.174, f32[8,2,64]{2,1,0:T(2,128)} %get-tuple-element.59, f32[8,64,2]{2,1,0:T(8,128)} %copy.63, f32[8,2,64]{2,1,0:T(2,128)} %get-tuple-element.44, f32[8,64,2]{2,1,0:T(8,128)} %bitcast.695, f32[8,2,64]{2,1,0:T(2,128)} %get-tuple-element.28, ...), kind=kLoop, calls=%fused_computation.49 | loop fusion | flops 3145728 | bytes 688192 | tf_op jit(solution)/shard_map/jit(_where)/select_n | solution.py:92
  256.5 10.7 %all_to_all.116 = bf16[8,8,8,128]{3,2,1,0:T(8,128)(2,1)} all-to-all(bf16[8,8,8,128]{3,2,1,0:T(8,128)(2,1)S(1)} %broadcast_in_dim.212), channel_id=1, replica_groups=mesh['grp'=2,'tp'=16,'dp_0'=4,'dp_1'=2] {'dp_0','dp_1'}, dimensions={0} | all-to-all | bytes 262144 | tf_op jit(solution)/shard_map/all_to_all | solution.py:23
  267.2 8.2 %all-to-all-start.8 = ((bf16[64,8,128]{2,1,0:T(8,128)(2,1)}), bf16[64,8,128]{2,1,0:T(8,128)(2,1)S(1)}, u32[]{:S(2)}, u32[]{:S(2)}) async-start(bf16[64,8,128]{2,1,0:T(8,128)(2,1)} %bitcast.157), calls=%async_computation.9 | async-start | bytes 262144 | tf_op jit(solution)/shard_map/all_to_all | solution.py:157
  275.5 14.2 %all-to-all-done.8 = bf16[64,8,128]{2,1,0:T(8,128)(2,1)S(1)} async-done(((bf16[64,8,128]{2,1,0:T(8,128)(2,1)}), bf16[64,8,128]{2,1,0:T(8,128)(2,1)S(1)}, u32[]{:S(2)}, u32[]{:S(2)}) %all-to-all-start.8) | async-done | bytes 131104 | tf_op jit(solution)/shard_map/all_to_all | solution.py:157
  291.9 53.7 %all_to_all.117 = f32[16,4,8,512]{3,2,1,0:T(8,128)S(1)} all-to-all(f32[16,4,8,512]{3,2,1,0:T(8,128)S(1)} %broadcast_in_dim.213), channel_id=1, replica_groups=mesh['grp'=2,'tp'=16,'dp_0'=4,'dp_1'=2] {'tp'}, dimensions={0} | all-to-all | bytes 2097152 | tf_op jit(solution)/shard_map/all_to_all | solution.py:23
  348.6 3.6 all-to-all-start.10
  353.2 6.3 %all-to-all-done.10 = f32[8,8,8,128]{3,2,1,0:T(8,128)S(1)} async-done(((f32[8,8,8,128]{3,2,1,0:T(8,128)}), f32[8,8,8,128]{3,2,1,0:T(8,128)S(1)}, u32[]{:S(2)}, u32[]{:S(2)}) %all-to-all-start.10) | async-done | bytes 262176 | tf_op jit(solution)/shard_map/all_to_all | solution.py:53
  359.5 3.6 all-to-all-start.14
  365.1 5.3 all-to-all-done.14
  370.4 3.6 all-to-all-start.13
  376.0 5.4 all-to-all-done.13
  381.4 4.2 all-to-all-start.12
  387.5 5.4 all-to-all-done.12
  393.0 4.4 all-to-all-start.11
  399.4 2.7 all-reduce.1
  404.8 4.2 all-to-all-start.15
  424.6 3.2 add_select_fusion.6
  432.5 5.6 add_select_fusion.5
  442.7 6.5 %add_select_fusion.4 = f32[8,64,2,64]{3,2,1,0:T(2,128)S(1)} fusion(pred[8]{0:T(512)(128)(4,1)} %get-tuple-element.178, f32[8,2,64]{2,1,0:T(2,128)S(1)} %get-tuple-element.103, f32[8,64,2]{2,1,0:T(8,128)} %copy.68, f32[8,2,64]{2,1,0:T(2,128)} %get-tuple-element.88, f32[8,64,2]{2,1,0:T(8,128)} %bitcast.665, f32[8,2,64]{2,1,0:T(2,128)} %get-tuple-element.72, ...), kind=kLoop, calls=%fused_computation.45 | loop fusion | flops 1572864 | bytes 606240 | tf_op jit(solution)/shard_map/jit(_where)/select_n | solution.py:92
  453.8 7.4 %add_select_fusion.3 = f32[8,64,2,64]{3,2,1,0:T(2,128)S(1)} fusion(pred[8]{0:T(512)(128)(4,1)} %get-tuple-element.177, f32[8,2,64]{2,1,0:T(2,128)} %get-tuple-element.104, f32[8,64,2]{2,1,0:T(8,128)} %copy.69, f32[8,2,64]{2,1,0:T(2,128)} %get-tuple-element.89, f32[8,64,2]{2,1,0:T(8,128)} %bitcast.676, f32[8,2,64]{2,1,0:T(2,128)} %get-tuple-element.73, ...), kind=kLoop, calls=%fused_computation.44 | loop fusion | flops 1966080 | bytes 626728 | tf_op jit(solution)/shard_map/jit(_where)/select_n | solution.py:92
  465.9 9.1 %add_select_fusion.2 = f32[8,64,2,64]{3,2,1,0:T(2,128)S(1)} fusion(pred[8]{0:T(512)(128)(4,1)} %get-tuple-element.176, f32[8,2,64]{2,1,0:T(2,128)} %get-tuple-element.105, f32[8,64,2]{2,1,0:T(8,128)} %copy.70, f32[8,2,64]{2,1,0:T(2,128)} %get-tuple-element.90, f32[8,64,2]{2,1,0:T(8,128)} %bitcast.685, f32[8,2,64]{2,1,0:T(2,128)} %get-tuple-element.74, ...), kind=kLoop, calls=%fused_computation.43 | loop fusion | flops 2359296 | bytes 647216 | tf_op jit(solution)/shard_map/jit(_where)/select_n | solution.py:92
  479.6 10.0 %add_select_fusion.1 = f32[8,64,2,64]{3,2,1,0:T(2,128)S(1)} fusion(pred[8]{0:T(512)(128)(4,1)} %get-tuple-element.175, f32[8,2,64]{2,1,0:T(2,128)} %get-tuple-element.106, f32[8,64,2]{2,1,0:T(8,128)} %copy.71, f32[8,2,64]{2,1,0:T(2,128)} %get-tuple-element.91, f32[8,64,2]{2,1,0:T(8,128)} %bitcast.692, f32[8,2,64]{2,1,0:T(2,128)} %get-tuple-element.75, ...), kind=kLoop, calls=%fused_computation.42 | loop fusion | flops 2752512 | bytes 667704 | tf_op jit(solution)/shard_map/jit(_where)/select_n | solution.py:92
  502.0 11.2 %add_select_fusion = f32[8,64,2,64]{3,2,1,0:T(2,128)S(1)} fusion(pred[8]{0:T(512)(128)(4,1)} %get-tuple-element.174, f32[8,2,64]{2,1,0:T(2,128)} %get-tuple-element.107, f32[8,64,2]{2,1,0:T(8,128)} %copy.72, f32[8,2,64]{2,1,0:T(2,128)} %get-tuple-element.92, f32[8,64,2]{2,1,0:T(8,128)} %bitcast.697, f32[8,2,64]{2,1,0:T(2,128)} %get-tuple-element.76, ...), kind=kLoop, calls=%fused_computation.41 | loop fusion | flops 3145728 | bytes 688192 | tf_op jit(solution)/shard_map/jit(_where)/select_n | solution.py:92
  525.7 4.6 all-to-all-start.16
  564.5 7.3 %all-to-all-start.17 = ((bf16[64,8,128]{2,1,0:T(8,128)(2,1)}), bf16[64,8,128]{2,1,0:T(8,128)(2,1)}, u32[]{:S(2)}, u32[]{:S(2)}) async-start(bf16[64,8,128]{2,1,0:T(8,128)(2,1)} %bitcast.310), calls=%async_computation.19 | async-start | bytes 262144 | tf_op jit(solution)/shard_map/all_to_all | solution.py:157
  572.2 3.4 add_select_fusion.17
  606.9 2.3 add_select_fusion.16
  610.1 2.8 fusion.7
  (586 shorter events, 214.1 us)
Async XLA Ops:
  8.0 26.1 %copy-start.127 = (f32[2,512]{1,0:T(2,128)S(1)}, f32[2,512]{1,0:T(2,128)}, u32[]{:S(2)}) copy-start(f32[2,512]{1,0:T(2,128)} %param.15) | copy-start | bytes 12292
  9.9 74.9 %copy-start.42 = (bf16[2,128,512]{2,1,0:T(8,128)(2,1)S(1)}, bf16[2,128,512]{2,1,0:T(8,128)(2,1)}, u32[]{:S(2)}) copy-start(bf16[2,128,512]{2,1,0:T(8,128)(2,1)} %param.22) | copy-start | bytes 786436
  9.9 75.7 %copy-start.131 = (s32[64]{0:T(128)S(1)}, s32[64]{0:T(128)}, u32[]{:S(2)}) copy-start(s32[64]{0:T(128)} %param.14) | copy-start | bytes 772
  9.9 77.0 %copy-start.128 = (f32[2,128]{1,0:T(2,128)S(1)}, f32[2,128]{1,0:T(2,128)}, u32[]{:S(2)}) copy-start(f32[2,128]{1,0:T(2,128)} %param.23) | copy-start | bytes 3076
  9.9 77.7 %copy-start.129 = (f32[2,128]{1,0:T(2,128)S(1)}, f32[2,128]{1,0:T(2,128)}, u32[]{:S(2)}) copy-start(f32[2,128]{1,0:T(2,128)} %param.24) | copy-start | bytes 3076
  9.9 78.3 %copy-start.27 = (f32[2,8,64,128]{3,2,1,0:T(8,128)S(1)}, f32[2,8,64,128]{3,2,1,0:T(8,128)}, u32[]{:S(2)}) copy-start(f32[2,8,64,128]{3,2,1,0:T(8,128)} %param.25) | copy-start | bytes 1572868
  9.9 73.9 %all-to-all-start = ((f32[16,4,8,512]{3,2,1,0:T(8,128)}), f32[16,4,8,512]{3,2,1,0:T(8,128)S(1)}, u32[]{:S(2)}, u32[]{:S(2)}) async-start(f32[16,4,8,512]{3,2,1,0:T(8,128)} %broadcast_in_dim.196), calls=%async_computation | async-start | bytes 2097152 | tf_op jit(solution)/shard_map/all_to_all | solution.py:23
  34.1 107.1 %reduce-scatter.3.cloned.1.call-start = ((), (), s32[]{:S(2)}) async-start(), calls=%async_computation.20 | async-start | bytes 40960 | tf_op jit(solution)/shard_map/reduce_scatter | solution.py:41
  84.8 190.7 %all-gather.5.cloned.1.call-start = ((), (), s32[]{:S(2)}) async-start(), calls=%async_computation.22 | async-start | bytes 2228224 | tf_op jit(solution)/shard_map/all_gather | solution.py:161
  87.0 71.6 %copy-start.43 = (pred[8]{0:T(512)(128)(4,1)}, pred[8]{0:T(512)(128)(4,1)S(1)}, u32[]{:S(2)}) copy-start(pred[8]{0:T(512)(128)(4,1)S(1)} %get-tuple-element.181) | copy-start | bytes 28
  90.6 27.7 %copy-start.39 = (bf16[2,512,128]{2,1,0:T(8,128)(2,1)S(1)}, bf16[2,512,128]{2,1,0:T(8,128)(2,1)}, u32[]{:S(2)}) copy-start(bf16[2,512,128]{2,1,0:T(8,128)(2,1)} %param.20) | copy-start | bytes 786436
  91.6 12.1 %all-to-all-start.1 = ((f32[8,8,8,128]{3,2,1,0:T(8,128)}), f32[8,8,8,128]{3,2,1,0:T(8,128)S(1)}, u32[]{:S(2)}, u32[]{:S(2)}) async-start(f32[8,8,8,128]{3,2,1,0:T(8,128)} %fusion.32), calls=%async_computation.1 | async-start | bytes 524288 | tf_op jit(solution)/shard_map/all_to_all | solution.py:53
  96.2 33.0 %copy-start.40 = (bf16[2,512,128]{2,1,0:T(8,128)(2,1)S(1)}, bf16[2,512,128]{2,1,0:T(8,128)(2,1)}, u32[]{:S(2)}) copy-start(bf16[2,512,128]{2,1,0:T(8,128)(2,1)} %param.17) | copy-start | bytes 786436
  103.8 10.9 %all-to-all-start.5 = ((f32[8,8,8,128]{3,2,1,0:T(8,128)}), f32[8,8,8,128]{3,2,1,0:T(8,128)S(1)}, u32[]{:S(2)}, u32[]{:S(2)}) async-start(f32[8,8,8,128]{3,2,1,0:T(8,128)} %fusion.24), calls=%async_computation.6 | async-start | bytes 524288 | tf_op jit(solution)/shard_map/all_to_all | solution.py:53
  107.4 32.7 %copy-start.41 = (bf16[2,512,128]{2,1,0:T(8,128)(2,1)S(1)}, bf16[2,512,128]{2,1,0:T(8,128)(2,1)}, u32[]{:S(2)}) copy-start(bf16[2,512,128]{2,1,0:T(8,128)(2,1)} %param.21) | copy-start | bytes 786436
  114.7 10.9 %all-to-all-start.4 = ((f32[8,8,8,128]{3,2,1,0:T(8,128)}), f32[8,8,8,128]{3,2,1,0:T(8,128)S(1)}, u32[]{:S(2)}, u32[]{:S(2)}) async-start(f32[8,8,8,128]{3,2,1,0:T(8,128)} %fusion.26), calls=%async_computation.5 | async-start | bytes 524288 | tf_op jit(solution)/shard_map/all_to_all | solution.py:53
  125.6 10.9 %all-to-all-start.3 = ((f32[8,8,8,128]{3,2,1,0:T(8,128)}), f32[8,8,8,128]{3,2,1,0:T(8,128)S(1)}, u32[]{:S(2)}, u32[]{:S(2)}) async-start(f32[8,8,8,128]{3,2,1,0:T(8,128)} %fusion.28), calls=%async_computation.4 | async-start | bytes 524288 | tf_op jit(solution)/shard_map/all_to_all | solution.py:53
  136.5 10.9 %all-to-all-start.2 = ((f32[8,8,8,128]{3,2,1,0:T(8,128)}), f32[8,8,8,128]{3,2,1,0:T(8,128)S(1)}, u32[]{:S(2)}, u32[]{:S(2)}) async-start(f32[8,8,8,128]{3,2,1,0:T(8,128)} %fusion.30), calls=%async_computation.3 | async-start | bytes 524288 | tf_op jit(solution)/shard_map/all_to_all | solution.py:53
  147.4 107.3 %all-to-all-start.6 = ((f32[8,8,8,128]{3,2,1,0:T(8,128)}), f32[8,8,8,128]{3,2,1,0:T(8,128)}, u32[]{:S(2)}, u32[]{:S(2)}) async-start(f32[8,8,8,128]{3,2,1,0:T(8,128)} %fusion.22), calls=%async_computation.7 | async-start | bytes 524288 | tf_op jit(solution)/shard_map/all_to_all | solution.py:53
  156.1 79.9 %copy-start.1 = (f32[8,64,2]{2,1,0:T(8,128)}, f32[8,64,2]{2,1,0:T(8,128)S(1)}, u32[]{:S(2)}) copy-start(f32[8,64,2]{2,1,0:T(8,128)S(1)} %copy.59) | copy-start | bytes 12292
  156.3 79.8 %copy-start.7 = (f32[8,64,2]{2,1,0:T(8,128)}, f32[8,64,2]{2,1,0:T(8,128)S(1)}, u32[]{:S(2)}) copy-start(f32[8,64,2]{2,1,0:T(8,128)S(1)} %copy.60) | copy-start | bytes 12292
  156.4 79.6 %copy-start.13 = (f32[8,64,2]{2,1,0:T(8,128)}, f32[8,64,2]{2,1,0:T(8,128)S(1)}, u32[]{:S(2)}) copy-start(f32[8,64,2]{2,1,0:T(8,128)S(1)} %copy.61) | copy-start | bytes 12292
  180.4 55.6 %copy-start.3 = (f32[8,2,1,64]{1,3,0,2:T(8,128)}, f32[8,2,1,64]{1,3,0,2:T(8,128)S(1)}, u32[]{:S(2)}) copy-start(f32[8,2,1,64]{1,3,0,2:T(8,128)S(1)} %copy.99) | copy-start | bytes 12292
  191.0 45.0 %copy-start.9 = (f32[8,2,1,64]{1,3,0,2:T(8,128)}, f32[8,2,1,64]{1,3,0,2:T(8,128)S(1)}, u32[]{:S(2)}) copy-start(f32[8,2,1,64]{1,3,0,2:T(8,128)S(1)} %copy.104) | copy-start | bytes 12292
  247.2 42.5 %copy-start.47 = (bf16[4,8,512]{2,1,0:T(8,128)(2,1)S(1)}, bf16[4,8,512]{2,1,0:T(8,128)(2,1)}, u32[]{:S(2)}) copy-start(bf16[4,8,512]{2,1,0:T(8,128)(2,1)} %param.13) | copy-start | bytes 98308
  267.2 22.4 %all-to-all-start.8 = ((bf16[64,8,128]{2,1,0:T(8,128)(2,1)}), bf16[64,8,128]{2,1,0:T(8,128)(2,1)S(1)}, u32[]{:S(2)}, u32[]{:S(2)}) async-start(bf16[64,8,128]{2,1,0:T(8,128)(2,1)} %bitcast.157), calls=%async_computation.9 | async-start | bytes 262144 | tf_op jit(solution)/shard_map/all_to_all | solution.py:157
  275.4 124.0 %reduce-scatter.5.cloned.1.call-start = ((), (), s32[]{:S(2)}) async-start(), calls=%async_computation.21 | async-start | bytes 40960 | tf_op jit(solution)/shard_map/reduce_scatter | solution.py:41
  291.7 53.9 %copy-start.126 = (f32[1,512]{1,0:T(1,128)S(1)}, f32[1,512]{1,0:T(1,128)}, u32[]{:S(2)}) copy-start(f32[1,512]{1,0:T(1,128)} %get-tuple-element.167) | copy-start | bytes 6148
  291.8 55.3 %copy-start.130 = (f32[128]{0:T(128)S(1)}, f32[128]{0:T(128)}, u32[]{:S(2)}) copy-start(f32[128]{0:T(128)} %get-tuple-element.2) | copy-start | bytes 1540
  291.8 55.4 %copy-start.32 = (f32[1,8,64,128]{3,2,1,0:T(8,128)S(1)}, f32[1,8,64,128]{3,2,1,0:T(8,128)}, u32[]{:S(2)}) copy-start(f32[1,8,64,128]{3,2,1,0:T(8,128)} %get-tuple-element.16) | copy-start | bytes 786436
  291.9 55.7 %copy-start.35 = (bf16[2,512,128]{2,1,0:T(8,128)(2,1)S(1)}, bf16[2,512,128]{2,1,0:T(8,128)(2,1)}, u32[]{:S(2)}) copy-start(bf16[2,512,128]{2,1,0:T(8,128)(2,1)} %param.19) | copy-start | bytes 786436
  346.5 263.6 %all-gather.7.cloned.1.call-start = ((), (), s32[]{:S(2)}) async-start(), calls=%async_computation.23 | async-start | bytes 2228224 | tf_op jit(solution)/shard_map/all_gather | solution.py:161
  348.6 11.0 %all-to-all-start.10 = ((f32[8,8,8,128]{3,2,1,0:T(8,128)}), f32[8,8,8,128]{3,2,1,0:T(8,128)S(1)}, u32[]{:S(2)}, u32[]{:S(2)}) async-start(f32[8,8,8,128]{3,2,1,0:T(8,128)} %fusion.20), calls=%async_computation.11 | async-start | bytes 524288 | tf_op jit(solution)/shard_map/all_to_all | solution.py:53
  359.5 10.9 %all-to-all-start.14 = ((f32[8,8,8,128]{3,2,1,0:T(8,128)}), f32[8,8,8,128]{3,2,1,0:T(8,128)S(1)}, u32[]{:S(2)}, u32[]{:S(2)}) async-start(f32[8,8,8,128]{3,2,1,0:T(8,128)} %fusion.12), calls=%async_computation.16 | async-start | bytes 524288 | tf_op jit(solution)/shard_map/all_to_all | solution.py:53
  370.4 10.9 %all-to-all-start.13 = ((f32[8,8,8,128]{3,2,1,0:T(8,128)}), f32[8,8,8,128]{3,2,1,0:T(8,128)S(1)}, u32[]{:S(2)}, u32[]{:S(2)}) async-start(f32[8,8,8,128]{3,2,1,0:T(8,128)} %fusion.14), calls=%async_computation.15 | async-start | bytes 524288 | tf_op jit(solution)/shard_map/all_to_all | solution.py:53
  381.4 11.6 %all-to-all-start.12 = ((f32[8,8,8,128]{3,2,1,0:T(8,128)}), f32[8,8,8,128]{3,2,1,0:T(8,128)}, u32[]{:S(2)}, u32[]{:S(2)}) async-start(f32[8,8,8,128]{3,2,1,0:T(8,128)} %fusion.16), calls=%async_computation.14 | async-start | bytes 524288 | tf_op jit(solution)/shard_map/all_to_all | solution.py:53
  393.0 11.8 %all-to-all-start.11 = ((f32[8,8,8,128]{3,2,1,0:T(8,128)}), f32[8,8,8,128]{3,2,1,0:T(8,128)}, u32[]{:S(2)}, u32[]{:S(2)}) async-start(f32[8,8,8,128]{3,2,1,0:T(8,128)} %fusion.18), calls=%async_computation.13 | async-start | bytes 524288 | tf_op jit(solution)/shard_map/all_to_all | solution.py:53
  404.8 118.5 %all-to-all-start.15 = ((f32[8,8,8,128]{3,2,1,0:T(8,128)}), f32[8,8,8,128]{3,2,1,0:T(8,128)}, u32[]{:S(2)}, u32[]{:S(2)}) async-start(f32[8,8,8,128]{3,2,1,0:T(8,128)} %fusion.10), calls=%async_computation.17 | async-start | bytes 524288 | tf_op jit(solution)/shard_map/all_to_all | solution.py:53
  513.5 19.9 %copy-start.92 = (f32[8,1,2,64]{3,2,1,0:T(2,128)S(1)}, f32[8,1,2,64]{3,2,1,0:T(2,128)}, u32[]{:S(2)}) copy-start(f32[8,1,2,64]{3,2,1,0:T(2,128)} %get-tuple-element.20) | copy-start | bytes 12292
  513.5 20.6 %copy-start.91 = (f32[8,1,2,64]{3,2,1,0:T(2,128)S(1)}, f32[8,1,2,64]{3,2,1,0:T(2,128)}, u32[]{:S(2)}) copy-start(f32[8,1,2,64]{3,2,1,0:T(2,128)} %get-tuple-element.29) | copy-start | bytes 12292
  513.5 21.3 %copy-start.90 = (f32[8,1,2,64]{3,2,1,0:T(2,128)S(1)}, f32[8,1,2,64]{3,2,1,0:T(2,128)}, u32[]{:S(2)}) copy-start(f32[8,1,2,64]{3,2,1,0:T(2,128)} %get-tuple-element.30) | copy-start | bytes 12292
  513.5 21.9 %copy-start.89 = (f32[8,1,2,64]{3,2,1,0:T(2,128)S(1)}, f32[8,1,2,64]{3,2,1,0:T(2,128)}, u32[]{:S(2)}) copy-start(f32[8,1,2,64]{3,2,1,0:T(2,128)} %get-tuple-element.31) | copy-start | bytes 12292
  513.5 22.6 %copy-start.88 = (f32[8,1,2,64]{3,2,1,0:T(2,128)S(1)}, f32[8,1,2,64]{3,2,1,0:T(2,128)}, u32[]{:S(2)}) copy-start(f32[8,1,2,64]{3,2,1,0:T(2,128)} %get-tuple-element.32) | copy-start | bytes 12292
  513.5 23.2 %copy-start.87 = (f32[8,1,2,64]{3,2,1,0:T(2,128)S(1)}, f32[8,1,2,64]{3,2,1,0:T(2,128)}, u32[]{:S(2)}) copy-start(f32[8,1,2,64]{3,2,1,0:T(2,128)} %get-tuple-element.33) | copy-start | bytes 12292
  513.5 23.9 %copy-start.86 = (f32[8,1,2,64]{3,2,1,0:T(2,128)S(1)}, f32[8,1,2,64]{3,2,1,0:T(2,128)}, u32[]{:S(2)}) copy-start(f32[8,1,2,64]{3,2,1,0:T(2,128)} %get-tuple-element.34) | copy-start | bytes 12292
  513.5 24.6 %copy-start.85 = (f32[8,1,2,64]{3,2,1,0:T(2,128)S(1)}, f32[8,1,2,64]{3,2,1,0:T(2,128)}, u32[]{:S(2)}) copy-start(f32[8,1,2,64]{3,2,1,0:T(2,128)} %get-tuple-element.35) | copy-start | bytes 12292
  525.7 38.8 %all-to-all-start.16 = ((bf16[8,8,8,128]{3,2,1,0:T(8,128)(2,1)}), bf16[8,8,8,128]{3,2,1,0:T(8,128)(2,1)}, u32[]{:S(2)}, u32[]{:S(2)}) async-start(bf16[8,8,8,128]{3,2,1,0:T(8,128)(2,1)} %broadcast_in_dim.214), calls=%async_computation.18 | async-start | bytes 262144 | tf_op jit(solution)/shard_map/all_to_all | solution.py:23
  564.5 45.6 %all-to-all-start.17 = ((bf16[64,8,128]{2,1,0:T(8,128)(2,1)}), bf16[64,8,128]{2,1,0:T(8,128)(2,1)}, u32[]{:S(2)}, u32[]{:S(2)}) async-start(bf16[64,8,128]{2,1,0:T(8,128)(2,1)} %bitcast.310), calls=%async_computation.19 | async-start | bytes 262144 | tf_op jit(solution)/shard_map/all_to_all | solution.py:157
  (105 other events, 874.8 us)
Sparse Core Ops, SparseCore 0:
  84.9 23.9 reduce-scatter.2
  346.6 21.2 reduce-scatter.4
Sparse Core Ops, SparseCore 1:
  87.1 68.4 all-gather.4
  348.8 65.4 all-gather.6
where the time goes:
time: 632 us; the launch traced here: 621 us
  local copies, waits for them, and re-layouts  132 us (21%)
  other arithmetic  125 us (20%)
  waiting for transfers between devices  116 us (18%)
  starting transfers between devices  91.7 us (15%)
  blocking collectives  69.7 us (11%)
  matrix products  67.3 us (11%)
  between operations  18.8 us (3%)
    select_n x18, other arithmetic, mix_heads(): jnp.where(live_mask[:, position][:, None, None, None], updated, memory)  112 us
    all_to_all x2, blocking collectives, from_everyone(): lax.all_to_all(jnp.broadcast_to(value[None], (size, *value.shape)), axis,...  64.4 us
    all_to_all x12, waiting for transfers between devices, sum_at_owner(): blocks = lax.all_to_all(cut_along(value, dim, size), axis, 0, 0, tiled=True)  52.3 us
    all_to_all x2, waiting for transfers between devices, from_everyone(): lax.all_to_all(jnp.broadcast_to(value[None], (size, *value.shape)), axis,...  49.2 us
    all_to_all x12, starting transfers between devices, sum_at_owner(): blocks = lax.all_to_all(cut_along(value, dim, size), axis, 0, 0, tiled=True)  47.2 us
    all_to_all x2, starting transfers between devices, from_everyone(): lax.all_to_all(jnp.broadcast_to(value[None], (size, *value.shape)), axis,...  28.7 us
    mul x48, local copies, waits for them, and re-layouts, mix_heads(): jnp.swapaxes(value_heads[:, position], 1, 2)[:, :, :, None]  28.1 us
    mul x48, local copies, waits for them, and re-layouts, mix_heads(): jnp.swapaxes(seen_part, 1, 2)[:, :, :, None]  25.9 us
  transfers between devices with their start and end apart: 20, of which 12 were waited for; matrix products, arithmetic and copies ran while one was open for 51% of the time, Pallas kernels for 0%

commit v1 on v0

v1 whole, which is shorter than its diff:
```python
import functools

import jax
import jax.numpy as jnp
from jax import lax
from jax.experimental import pallas as pl
from jax.experimental.pallas import tpu as pltpu
from jax.sharding import Mesh
from jax.sharding import PartitionSpec as P

D = 4096
HEAD = 64
BLOCKS = 2
LANES = 128
CORES = 2
LIVE = 224
SLOTS = 16
DP = ("x", "c")
GRP_DP = ("grp", "x", "c")

group_eps = 0.00064
norm_eps = 1e-06
key_eps = 1e-06
decay_scale = 0.606531

f32 = jnp.float32
bf16 = jnp.bfloat16


def iota(shape, dim):
    return lax.broadcasted_iota(jnp.int32, shape, dim)


def vmem():
    return pl.BlockSpec(memory_space=pltpu.VMEM)


def smem():
    return pl.BlockSpec(memory_space=pltpu.SMEM)


def call(kernel, out_shape, in_specs, out_specs=None, scratch=(), **more):
    if out_specs is None:
        out_specs = jax.tree.map(lambda _: vmem(), out_shape)
    return pl.pallas_call(
        kernel,
        grid=(1,),
        out_shape=out_shape,
        in_specs=in_specs,
        out_specs=out_specs,
        scratch_shapes=list(scratch),
        **more,
    )


def split_two(value):
    high = value.astype(bf16)
    low = (value - high.astype(f32)).astype(bf16)
    return jnp.concatenate([high, low], axis=1)


def head_mask():
    rows, cols = iota((2 * LANES, LANES), 0), iota((2 * LANES, LANES), 1)
    return jnp.where((rows % LANES) // HEAD == cols // HEAD, 1.0, 0.0).astype(bf16)


def head_sum(value, mask):
    return jnp.dot(split_two(value), mask, preferred_element_type=f32)


def compact_rows(lens, slots, rows, steps, first):
    seqs = rows // steps
    seq_of = iota((seqs, rows), 1) // steps
    before = jnp.where(iota((seqs, rows), 0) < seq_of, 1.0, 0.0).astype(bf16)
    same = jnp.where(iota((seqs, rows), 0) == seq_of, 1.0, 0.0).astype(bf16)
    wide = jnp.broadcast_to(lens.astype(f32), (8, seqs)).astype(bf16)
    start = jnp.dot(wide, before, preferred_element_type=f32)[0:1]
    count = jnp.dot(wide, same, preferred_element_type=f32)[0:1]
    step = (iota((1, rows), 1) % steps).astype(f32)
    place = jnp.where(step < count, start + step, -1.0)
    slot = (iota((slots, rows), 0) + first).astype(f32)
    return jnp.where(slot == jnp.broadcast_to(place, (slots, rows)), 1.0, 0.0).astype(bf16)


def spread_rows(lens, rows, slots, steps):
    seqs = rows // steps
    wide = jnp.broadcast_to(lens.astype(f32), (rows, seqs))
    seq_of = iota((rows, seqs), 0) // steps
    start = jnp.sum(jnp.where(iota((rows, seqs), 1) < seq_of, wide, 0.0), axis=1, keepdims=True)
    count = jnp.sum(jnp.where(iota((rows, seqs), 1) == seq_of, wide, 0.0), axis=1, keepdims=True)
    step = (iota((rows, 1), 0) % steps).astype(f32)
    live = step < count
    place = jnp.where(live, start + step, -1.0)
    slot = iota((rows, slots), 1).astype(f32)
    return jnp.where(slot == jnp.broadcast_to(place, (rows, slots)), 1.0, 0.0).astype(bf16), live


def two_lanes(total):
    high = total.astype(bf16).astype(f32)
    return jnp.where(iota(total.shape, 1) < LANES // 2, high, total - high)


def project(index_ref, scaled, squares, weights, keep_ref, send_ref, scaled_scr, square_scr):
    owners = scaled_scr.shape[0]
    held = scaled_scr.shape[1]
    scaled_scr[...] = scaled.reshape(scaled_scr.shape)
    square_scr[...] = jnp.broadcast_to(squares, (owners * held, LANES)).reshape(square_scr.shape)
    weight = jnp.concatenate([w[0] for w in weights], axis=1)
    width = weight.shape[1]
    core = index_ref[0]
    for target, who in ((send_ref, 1 - core), (keep_ref, core)):
        left = jnp.concatenate([scaled_scr[CORES * x + who] for x in range(owners // CORES)], axis=0)
        part = jnp.dot(left, weight, preferred_element_type=f32)
        for x in range(owners // CORES):
            target[x, :, :width] = part[x * held : (x + 1) * held].astype(target.dtype)
            square = square_scr[CORES * x + who]
            if target is send_ref:
                square = two_lanes(square)
            else:
                square = jnp.where(iota(square.shape, 1) < LANES // 2, square, 0.0)
            target[x, :, width:] = square.astype(target.dtype)


def first_kernel(index_ref, tokens_ref, gain_ref, *refs):
    weights, (keep_ref, send_ref, scaled_scr, square_scr) = refs[:6], refs[6:]
    x = tokens_ref[...].astype(f32)
    scaled = (x * gain_ref[0:1]).astype(bf16)
    squares = jnp.sum(x * x, axis=1, keepdims=True)
    project(index_ref, scaled, squares, weights, keep_ref, send_ref, scaled_scr, square_scr)


def next_kernel(steps, index_ref, lens_ref, gathered_ref, tokens_ref, gain_ref, *refs):
    weights, (keep_ref, send_ref, resid_ref, scaled_scr, square_scr, wide_scr) = refs[:6], refs[6:]
    rows = scaled_scr.shape[0] * scaled_scr.shape[1]
    spread, live = spread_rows(lens_ref[...], rows, gathered_ref.shape[0], steps)
    wide = jnp.dot(spread, gathered_ref[...], preferred_element_type=f32)
    scaled = wide.astype(bf16)
    x = wide * (1.0 / gain_ref[1:2])
    squares = jnp.sum(x * x, axis=1, keepdims=True)
    own = resid_ref.shape[0]
    wide_scr[...] = jnp.where(live, x, 0.0).reshape(wide_scr.shape)
    live_own = jnp.where(live, 1.0, 0.0)
    square_scr[...] = jnp.broadcast_to(live_own, (rows, LANES)).reshape(square_scr.shape)
    rank = index_ref[1]
    chosen = wide_scr[rank]
    per = square_scr.shape[1] // own
    alive = square_scr[rank // per, pl.ds(pl.multiple_of((rank % per) * own, own), own), 0:1] > 0.5
    resid_ref[...] = jnp.where(alive, chosen, tokens_ref[...].astype(f32))
    project(index_ref, scaled, squares, weights, keep_ref, send_ref, scaled_scr, square_scr)


def add_kernel(keep_ref, got_ref, out_ref):
    width = out_ref.shape[2] - LANES
    total = keep_ref[...] + got_ref[...].astype(f32)
    out_ref[:, :, :width] = total[:, :, :width].astype(bf16)
    for x in range(out_ref.shape[0]):
        square = total[x, :, width:]
        square = square + pltpu.roll(square, LANES // 2, 1)
        out_ref[x, :, width:] = two_lanes(square).astype(bf16)


def mix_kernel(steps, index_ref, lens_ref, parts_ref, base_ref, gain_ref, state_ref, *refs):
    gated_ref, new_ref, rows_scr, seen_scr, value_scr, read_scr = refs[-6:]
    seqs = state_ref.shape[1]
    mask = head_mask()
    total = parts_ref[0].astype(f32)
    for x in range(1, parts_ref.shape[0]):
        total = total + parts_ref[x].astype(f32)
    square = total[:, 6 * LANES :]
    square = square + pltpu.roll(square, LANES // 2, 1)
    inv_rms = lax.rsqrt(square * (1.0 / D) + norm_eps)
    recept, keys, values, decay_pre, rate_pre, gate_pre = (
        total[:, i * LANES : (i + 1) * LANES] * inv_rms for i in range(6)
    )
    first = index_ref[2] * seqs
    live = jnp.concatenate(
        [iota((steps, LANES), 0) < lens_ref[first + b] for b in range(seqs)], axis=0
    )
    decay = jnp.exp(-decay_scale * jax.nn.sigmoid(decay_pre + base_ref[...]))
    rate = jax.nn.sigmoid(rate_pre)
    unit = keys * lax.rsqrt(head_sum(keys * keys, mask) + key_eps)
    rows_scr[0] = unit
    rows_scr[1] = jnp.where(live, decay, 1.0)
    rows_scr[2] = jnp.where(live, unit * rate, 0.0)
    rows_scr[3] = jnp.where(live, keys, 0.0)
    rows_scr[4] = values
    rows_scr[5] = recept
    diagonal = iota((HEAD, LANES), 0) == iota((HEAD, LANES), 1) % HEAD

    def row(which, b, s):
        return rows_scr[which, pl.ds(b * steps + s, 1), :]

    def widened(s):
        return [jnp.where(diagonal, row(4, b, s), 0.0) for b in range(seqs)]

    left = [state_ref[0, b] * row(0, b, 0) for b in range(seqs)] + widened(0)
    sums = head_sum(jnp.concatenate(left, axis=0), mask)
    span = seqs * HEAD
    seen_scr[...] = sums[:span].reshape(seen_scr.shape)
    value_scr[...] = sums[span:].reshape(value_scr.shape)
    new_ref[0] = state_ref[0]

    def step(s, carry):
        later = jnp.minimum(s + 1, steps - 1)
        ahead, now = [], []
        for b in range(seqs):
            state = (
                new_ref[0, b] * row(1, b, s)
                - seen_scr[b] * row(2, b, s)
                + value_scr[b] * row(3, b, s)
            )
            new_ref[0, b] = state
            ahead.append(state * row(0, b, later))
            now.append(state * row(5, b, s))
        sums = head_sum(jnp.concatenate(now + ahead + widened(later), axis=0), mask)
        for b in range(seqs):
            read = jnp.where(diagonal, sums[b * HEAD : (b + 1) * HEAD], 0.0)
            read_scr[pl.ds(b * steps + s, 1), :] = jnp.sum(read, axis=0, keepdims=True)
        seen_scr[...] = sums[span : 2 * span].reshape(seen_scr.shape)
        value_scr[...] = sums[2 * span :].reshape(value_scr.shape)
        return carry

    lax.fori_loop(0, steps, step, 0)
    read = read_scr[...]
    centered = read - head_sum(read, mask) * (1.0 / HEAD)
    spread = head_sum(centered * centered, mask) * (1.0 / HEAD)
    normed = centered * lax.rsqrt(spread + group_eps)
    gated = normed * gain_ref[...] * jax.nn.sigmoid(gate_pre)
    gated = jnp.where(live, gated, 0.0).astype(bf16)
    for d in range(gated_ref.shape[0]):
        gated_ref[d] = gated


def out_compact_kernel(steps, lens_ref, gated_ref, weight_ref, out_ref):
    slots = out_ref.shape[0] * out_ref.shape[1]
    pick = compact_rows(lens_ref[...], slots, gated_ref.shape[0], steps, 0)
    rows = jnp.dot(pick, gated_ref[...], preferred_element_type=f32).astype(bf16)
    part = jnp.dot(rows, weight_ref[0], preferred_element_type=f32)
    out_ref[...] = part.astype(bf16).reshape(out_ref.shape)


def out_kernel(gated_ref, weight_ref, out_ref):
    part = jnp.dot(gated_ref[...], weight_ref[0], preferred_element_type=f32)
    out_ref[...] = part.astype(bf16).reshape(out_ref.shape)


def join_kernel(steps, index_ref, lens_ref, tokens_ref, parts_ref, gain_ref, out_ref):
    slots = parts_ref.shape[1]
    pick = compact_rows(
        lens_ref[...], slots, tokens_ref.shape[0], steps, index_ref[1] * slots
    )
    x = jnp.dot(pick, tokens_ref[...], preferred_element_type=f32)
    total = parts_ref[0].astype(f32)
    for t in range(1, parts_ref.shape[0]):
        total = total + parts_ref[t].astype(f32)
    scaled = ((x + total) * gain_ref[1:2]).astype(bf16)
    for t in range(out_ref.shape[0]):
        out_ref[t] = scaled


def final_kernel(parts_ref, resid_ref, out_ref):
    total = parts_ref[0].astype(f32)
    for t in range(1, parts_ref.shape[0]):
        total = total + parts_ref[t].astype(f32)
    out_ref[...] = resid_ref[...] + total


def body(
    tokens,
    lengths,
    norm_gain,
    w_recept,
    w_key,
    w_value,
    w_decay,
    w_rate,
    w_gate,
    w_out,
    decay_base,
    out_gain,
    states,
):
    own_seqs, steps, feats = tokens.shape
    tp, xs = lax.axis_size("tp"), lax.axis_size("x")
    owners = xs * CORES
    own = own_seqs * steps
    rows = own * tp
    held = rows // owners
    seqs = states.shape[1]
    lanes = w_key.shape[2]
    width = 6 * lanes + LANES
    assert lanes == LANES and SLOTS * tp >= LIVE and seqs * steps == held

    index = jnp.stack([lax.axis_index("c"), lax.axis_index("tp"), lax.axis_index(DP)]).astype(
        jnp.int32
    )
    lens_row = lengths.reshape(1, -1)
    mine = tokens.reshape(own, feats)
    everyone = lax.all_gather(mine, "tp", axis=0, tiled=True)
    weights = (w_recept, w_key, w_value, w_decay, w_rate, w_gate)

    def pick(block, shape):
        return pl.BlockSpec((1, *shape), lambda _: (block, *(0 for _ in shape)))

    def weight_specs(block):
        return [pick(block, (feats, lanes)) for _ in weights]

    pair = (
        jax.ShapeDtypeStruct((xs, held, width), f32),
        jax.ShapeDtypeStruct((xs, held, width), bf16),
    )
    project_scratch = (
        pltpu.VMEM((owners, held, feats), bf16),
        pltpu.VMEM((owners, held, LANES), f32),
    )

    def exchange(keep, send):
        got = lax.ppermute(send, "c", [(0, 1), (1, 0)])
        both = call(
            add_kernel, jax.ShapeDtypeStruct((xs, held, width), bf16), [vmem(), vmem()]
        )(keep, got)
        return lax.all_to_all(both, "x", 0, 0, tiled=True)

    def mixed(block, parts, news):
        out_shape = (
            jax.ShapeDtypeStruct((owners, held, lanes), bf16),
            jax.ShapeDtypeStruct(states.shape, f32),
        )
        extra = [] if news is None else [news]
        gated, news = call(
            functools.partial(mix_kernel, steps),
            out_shape,
            [smem(), smem(), vmem(), vmem(), vmem(), pick(block, states.shape[1:])]
            + [pl.BlockSpec(memory_space=pl.ANY)] * len(extra),
            (vmem(), pick(block, states.shape[1:])),
            (
                pltpu.VMEM((6, held, LANES), f32),
                pltpu.VMEM((seqs, HEAD, LANES), f32),
                pltpu.VMEM((seqs, HEAD, LANES), f32),
                pltpu.VMEM((held, LANES), f32),
            ),
            input_output_aliases={6: 1} if extra else {},
        )(
            index,
            lengths,
            parts,
            decay_base[block].reshape(1, -1),
            out_gain[block].reshape(1, -1),
            states,
            *extra,
        )
        gathered = lax.all_to_all(gated, DP, 0, 0, tiled=True)
        return gathered.reshape(rows, lanes), news

    keep, send = call(
        first_kernel,
        pair,
        [smem(), vmem(), vmem(), *weight_specs(0)],
        scratch=project_scratch,
    )(index, everyone, norm_gain, *weights)
    gated, news = mixed(0, exchange(keep, send), None)
    partial = call(
        functools.partial(out_compact_kernel, steps),
        jax.ShapeDtypeStruct((tp, SLOTS, feats), bf16),
        [vmem(), vmem(), pick(0, (lanes, feats))],
    )(lens_row, gated, w_out)
    partial = lax.all_to_all(partial, "tp", 0, 0, tiled=True)
    scaled = call(
        functools.partial(join_kernel, steps),
        jax.ShapeDtypeStruct((tp, SLOTS, feats), bf16),
        [smem(), vmem(), vmem(), vmem(), vmem()],
    )(index, lens_row, everyone, partial, norm_gain)
    scaled = lax.all_to_all(scaled, "tp", 0, 0, tiled=True).reshape(tp * SLOTS, feats)
    keep, send, resid = call(
        functools.partial(next_kernel, steps),
        (*pair, jax.ShapeDtypeStruct((own, feats), f32)),
        [smem(), vmem(), vmem(), vmem(), vmem(), *weight_specs(1)],
        scratch=(*project_scratch, pltpu.VMEM((tp, own, feats), f32)),
    )(index, lens_row, scaled, mine, norm_gain, *weights)
    gated, news = mixed(1, exchange(keep, send), news)
    partial = call(
        out_kernel,
        jax.ShapeDtypeStruct((tp, own, feats), bf16),
        [vmem(), pick(1, (lanes, feats))],
    )(gated, w_out)
    partial = lax.all_to_all(partial, "tp", 0, 0, tiled=True)
    stream = call(final_kernel, jax.ShapeDtypeStruct((own, feats), f32), [vmem(), vmem()])(
        partial, resid
    )
    return stream.reshape(tokens.shape), news


def solution(mesh):
    split = Mesh(
        mesh.devices.reshape(
            mesh.shape["grp"], mesh.shape["tp"], mesh.shape["dp"] // CORES, CORES
        ),
        ("grp", "tp", "x", "c"),
    )
    return jax.shard_map(
        body,
        mesh=split,
        in_specs=(
            P(("grp", "tp"), None, DP),
            P("grp"),
            P(None, DP),
            P(None, DP, "tp"),
            P(None, DP, "tp"),
            P(None, DP, "tp"),
            P(None, DP, "tp"),
            P(None, DP, "tp"),
            P(None, DP, "tp"),
            P(None, "tp", DP),
            P(None, "tp"),
            P(None, "tp"),
            P(None, GRP_DP, None, "tp"),
        ),
        out_specs=(P(("grp", "tp"), None, DP), P(None, GRP_DP, None, "tp")),
        check_vma=False,
    )
```

time: 632 us -> 222 us (0.35); the launches traced: 621 us -> 221 us
  local copies, waits for them, and re-layouts: 132 us -> 2.92 us
  other arithmetic: 125 us -> 0.6 us
  waiting for transfers between devices: 116 us -> 12.5 us
  blocking collectives: 69.7 us -> 169 us
  starting transfers between devices: 91.7 us -> 4.72 us
  matrix products: 67.3 us -> 0 us
  Pallas kernels: 0 us -> 30.2 us
  between operations: 18.8 us -> 0.66 us
    select_n x18 -> x0, other arithmetic: 112 us -> none  [mix_heads(): jnp.where(live_mask[:, position][:, None, None, None], updated, memory)]
    all_to_all x16 -> x1, waiting for transfers between devices: 116 us -> 8.48 us  [exchange(): return lax.all_to_all(both, 'x', 0, 0, tiled=True)]
    all_to_all x16 -> x1, starting transfers between devices: 91.4 us -> 4.71 us  [exchange(): return lax.all_to_all(both, 'x', 0, 0, tiled=True)]
    dot_general x44 -> x0, matrix products: 67.3 us -> none  [the longest x16 24.5 us: mix_heads(): jnp.einsum('bihj,bhj->bhi', memory, recept_heads[:, position], precision=...]
    mul x117 -> x0, local copies, waits for them, and re-layouts: 65.7 us -> none  [the longest x48 28.1 us: mix_heads(): jnp.swapaxes(value_heads[:, position], 1, 2)[:, :, :, None]]
    all_gather x0 -> x1, blocking collectives: none -> 53.7 us  [body(): everyone = lax.all_gather(mine, 'tp', axis=0, tiled=True)]
    all_to_all x2 -> x6, blocking collectives: 64.4 us -> 116 us  [the longest x2 57.1 us: body(): partial = lax.all_to_all(partial, 'tp', 0, 0, tiled=True)]
    pallas_call x0 -> x10, Pallas kernels: none -> 30.2 us  [the longest x2 11.2 us: mixed(): call(functools.partial(mix_kernel, steps), out_shape, [smem(), smem(), vm...]
  transfers between devices with their start and end apart: 20 -> 3, of which waited for: 12 -> 3; matrix products, arithmetic and copies ran while one was open for 51% -> 0% of each run, Pallas kernels for 0% -> 0%
where the time goes in v1:
time: 222 us; the launch traced here: 221 us
  blocking collectives  169 us (76%)
  Pallas kernels  30.2 us (14%)
  waiting for transfers between devices  12.5 us (6%)
  starting transfers between devices  4.72 us (2%)
  local copies, waits for them, and re-layouts  2.92 us (1%)
    all_to_all x2, blocking collectives, body(): partial = lax.all_to_all(partial, 'tp', 0, 0, tiled=True)  57.1 us
    all_gather x1, blocking collectives, body(): everyone = lax.all_gather(mine, 'tp', axis=0, tiled=True)  53.7 us
    all_to_all x1, blocking collectives, body(): lax.all_to_all(scaled, 'tp', 0, 0, tiled=True).reshape(tp * SLOTS, feats)  24.7 us
    all_to_all x2, blocking collectives, mixed(): gathered = lax.all_to_all(gated, DP, 0, 0, tiled=True)  20.3 us
    all_to_all x1, blocking collectives, exchange(): return lax.all_to_all(both, 'x', 0, 0, tiled=True)  13.6 us
    pallas_call x2, Pallas kernels, mixed(): call(functools.partial(mix_kernel, steps), out_shape, [smem(), smem(), vm...  11.2 us
    all_to_all x1, waiting for transfers between devices, exchange(): return lax.all_to_all(both, 'x', 0, 0, tiled=True)  8.48 us
    all_to_all x1, starting transfers between devices, exchange(): return lax.all_to_all(both, 'x', 0, 0, tiled=True)  4.71 us
  transfers between devices with their start and end apart: 3, of which 3 were waited for; matrix products, arithmetic and copies ran while one was open for 0% of the time, Pallas kernels for 0%

profile of v1, /device:TPU:40, one launch (start us, length us, event | category | flops | bytes accessed | tf_op | source)
XLA Modules:
  0.0 221.0 jit_solution(3192450876033858406)
XLA Ops:
  0.6 53.7 %all_gather.3.tokens_ref = bf16[512,512]{1,0:T(8,128)(2,1)} all-gather(bf16[32,512]{1,0:T(8,128)(2,1)} %bitcast.12), channel_id=1, replica_groups=mesh['grp'=2,'tp'=16,'x'=4,'c'=2] {'tp'}, dimensions={0}, use_global_device_ids=true | all-gather | bytes 557056 | tf_op jit(solution)/shard_map/all_gather | solution.py:299
  54.4 0.6 pad_add_fusion.index_ref
  55.0 3.1 %shard_map.140 = (f32[4,64,896]{2,1,0:T(8,128)}, bf16[4,64,896]{2,1,0:T(8,128)(2,1)}) custom-call(s32[3]{0:T(128)} %pad_add_fusion.index_ref, bf16[512,512]{1,0:T(8,128)(2,1)} %all_gather.3.tokens_ref, f32[2,512]{1,0:T(2,128)} %gain_ref.5, bf16[2,512,128]{2,1,0:T(8,128)(2,1)} %refs_0_.3, bf16[2,512,128]{2,1,0:T(8,128)(2,1)} %refs_1_.3, ...), custom_call_target="tpu_custom_call" | custom-call | tf_op jit(solution)/shard_map/pallas_call | solution.py:355
  58.0 0.0 collective-permute-start
  58.0 2.0 collective-permute-done.got_ref
  60.1 0.0 copy-start.1
  60.1 0.8 copy-done.1
  60.8 2.3 %shard_map.141 = bf16[4,64,896]{2,1,0:T(8,128)(2,1)} custom-call(f32[4,64,896]{2,1,0:T(8,128)} %get-tuple-element.11.keep_ref, bf16[4,64,896]{2,1,0:T(8,128)(2,1)} %copy-done.1), custom_call_target="tpu_custom_call" | custom-call | tf_op jit(solution)/shard_map/pallas_call | solution.py:319
  63.1 0.0 copy-start.3
  63.1 0.0 copy-start.4
  63.1 4.7 %all-to-all-start = ((bf16[4,64,896]{2,1,0:T(8,128)(2,1)}), bf16[4,64,896]{2,1,0:T(8,128)(2,1)S(1)}, u32[]{:S(2)}, u32[]{:S(2)}) async-start(bf16[4,64,896]{2,1,0:T(8,128)(2,1)} %shard_map.141), calls=%async_computation | async-start | bytes 917504 | tf_op jit(solution)/shard_map/all_to_all | solution.py:322
  67.8 0.0 copy-done.3
  67.8 0.0 copy-done.4
  67.8 0.6 fusion
  68.4 8.5 %all-to-all-done.parts_ref = bf16[4,64,896]{2,1,0:T(8,128)(2,1)S(1)} async-done(((bf16[4,64,896]{2,1,0:T(8,128)(2,1)}), bf16[4,64,896]{2,1,0:T(8,128)(2,1)S(1)}, u32[]{:S(2)}, u32[]{:S(2)}) %all-to-all-start) | async-done | bytes 458784 | tf_op jit(solution)/shard_map/all_to_all | solution.py:322
  76.9 0.0 copy-start
  76.9 0.8 copy-done
  77.7 5.6 %shard_map.142 = (bf16[8,64,128]{2,1,0:T(8,128)(2,1)}, f32[2,8,64,128]{3,2,1,0:T(8,128)}) custom-call(s32[3]{0:T(128)} %pad_add_fusion.index_ref, s32[64]{0:T(128)} %lens_ref.3, bf16[4,64,896]{2,1,0:T(8,128)(2,1)} %copy-done, f32[1,128]{1,0:T(1,128)} %get-tuple-element.24.base_ref, f32[1,128]{1,0:T(1,128)} %get-tuple-element.21.gain_ref, ...), custom_call_target="tpu_custom_call" | custom-call | tf_op jit(solution)/shard_map/pallas_call | solution.py:330
  83.3 10.2 %all_to_all.35 = bf16[8,64,128]{2,1,0:T(8,128)(2,1)} all-to-all(bf16[8,64,128]{2,1,0:T(8,128)(2,1)} %get-tuple-element.13), channel_id=1, replica_groups=mesh['grp'=2,'tp'=16,'x'=4,'c'=2] {'x','c'}, dimensions={0} | all-to-all | bytes 262144 | tf_op jit(solution)/shard_map/all_to_all | solution.py:352
  93.4 2.2 shard_map.143
  95.6 22.3 %all_to_all.36.parts_ref = bf16[16,16,512]{2,1,0:T(8,128)(2,1)} all-to-all(bf16[16,16,512]{2,1,0:T(8,128)(2,1)} %shard_map.143), channel_id=1, replica_groups=mesh['grp'=2,'tp'=16,'x'=4,'c'=2] {'tp'}, dimensions={0} | all-to-all | bytes 524288 | tf_op jit(solution)/shard_map/all_to_all | solution.py:367
  117.9 2.1 shard_map.144
  120.0 24.7 %all_to_all.37 = bf16[16,16,512]{2,1,0:T(8,128)(2,1)} all-to-all(bf16[16,16,512]{2,1,0:T(8,128)(2,1)} %shard_map.144), channel_id=1, replica_groups=mesh['grp'=2,'tp'=16,'x'=4,'c'=2] {'tp'}, dimensions={0} | all-to-all | bytes 524288 | tf_op jit(solution)/shard_map/all_to_all | solution.py:373
  144.7 3.2 %shard_map.145 = (f32[4,64,896]{2,1,0:T(8,128)}, bf16[4,64,896]{2,1,0:T(8,128)(2,1)}, f32[32,512]{1,0:T(8,128)}) custom-call(s32[3]{0:T(128)} %pad_add_fusion.index_ref, s32[1,64]{1,0:T(1,128)} %bitcast.17, bf16[256,512]{1,0:T(8,128)(2,1)} %bitcast.9, bf16[32,512]{1,0:T(8,128)(2,1)} %bitcast.13, f32[2,512]{1,0:T(2,128)} %gain_ref.5, ...), custom_call_target="tpu_custom_call" | custom-call | tf_op jit(solution)/shard_map/pallas_call | solution.py:374
  148.0 0.0 collective-permute-start.1
  148.0 2.0 collective-permute-done.1.got_ref
  150.0 0.0 copy-start.2
  150.0 0.8 copy-done.2
  150.8 2.3 %shard_map.146 = bf16[4,64,896]{2,1,0:T(8,128)(2,1)} custom-call(f32[4,64,896]{2,1,0:T(8,128)} %get-tuple-element.14.keep_ref, bf16[4,64,896]{2,1,0:T(8,128)(2,1)} %copy-done.2), custom_call_target="tpu_custom_call" | custom-call | tf_op jit(solution)/shard_map/pallas_call | solution.py:319
  153.1 13.6 %all_to_all.38.parts_ref = bf16[4,64,896]{2,1,0:T(8,128)(2,1)} all-to-all(bf16[4,64,896]{2,1,0:T(8,128)(2,1)} %shard_map.146), channel_id=1, replica_groups=mesh['grp'=2,'tp'=16,'x'=4,'c'=2] {'x'}, dimensions={0} | all-to-all | bytes 917504 | tf_op jit(solution)/shard_map/all_to_all | solution.py:322
  166.6 5.6 %shard_map.147 = (bf16[8,64,128]{2,1,0:T(8,128)(2,1)}, f32[2,8,64,128]{3,2,1,0:T(8,128)}) custom-call(s32[3]{0:T(128)} %pad_add_fusion.index_ref, s32[64]{0:T(128)} %lens_ref.3, bf16[4,64,896]{2,1,0:T(8,128)(2,1)} %all_to_all.38.parts_ref, f32[1,128]{1,0:T(1,128)} %get-tuple-element.25.base_ref, ...), custom_call_target="tpu_custom_call", output_to_operand_aliasing={{1}: (6, {})} | custom-call | tf_op jit(solution)/shard_map/pallas_call | solution.py:330
  172.2 10.2 %all_to_all.39 = bf16[8,64,128]{2,1,0:T(8,128)(2,1)} all-to-all(bf16[8,64,128]{2,1,0:T(8,128)(2,1)} %get-tuple-element.17), channel_id=1, replica_groups=mesh['grp'=2,'tp'=16,'x'=4,'c'=2] {'x','c'}, dimensions={0} | all-to-all | bytes 262144 | tf_op jit(solution)/shard_map/all_to_all | solution.py:352
  182.4 2.0 shard_map.148
  184.4 34.9 %all_to_all.40.parts_ref = bf16[16,32,512]{2,1,0:T(8,128)(2,1)} all-to-all(bf16[16,32,512]{2,1,0:T(8,128)(2,1)} %shard_map.148), channel_id=1, replica_groups=mesh['grp'=2,'tp'=16,'x'=4,'c'=2] {'tp'}, dimensions={0} | all-to-all | bytes 1048576 | tf_op jit(solution)/shard_map/all_to_all | solution.py:386
  219.3 1.8 shard_map.149
Async XLA Ops:
  58.0 2.0 collective-permute-start
  60.1 0.8 copy-start.1
  63.1 4.7 %copy-start.3 = (f32[2,128]{1,0:T(2,128)S(1)}, f32[2,128]{1,0:T(2,128)}, u32[]{:S(2)}) copy-start(f32[2,128]{1,0:T(2,128)} %param.24) | copy-start | bytes 3076
  63.1 4.7 %copy-start.4 = (f32[2,128]{1,0:T(2,128)S(1)}, f32[2,128]{1,0:T(2,128)}, u32[]{:S(2)}) copy-start(f32[2,128]{1,0:T(2,128)} %param.23) | copy-start | bytes 3076
  63.1 13.8 %all-to-all-start = ((bf16[4,64,896]{2,1,0:T(8,128)(2,1)}), bf16[4,64,896]{2,1,0:T(8,128)(2,1)S(1)}, u32[]{:S(2)}, u32[]{:S(2)}) async-start(bf16[4,64,896]{2,1,0:T(8,128)(2,1)} %shard_map.141), calls=%async_computation | async-start | bytes 917504 | tf_op jit(solution)/shard_map/all_to_all | solution.py:322
  76.9 0.8 copy-start
  148.0 2.0 collective-permute-start.1
  150.0 0.8 copy-start.2
